TPU v7x, 32 devices: a whole 2x2x4 slice. The times are simulated.
32 devices in a mesh: fs: 16 (over z, y, x), tp: 2 (over core).
Axes of the slice: x: 2, y: 2, z: 4, core: 2. Of those that a mesh axis runs over, the one named last changes fastest.
Arguments:
- tokens: bfloat16 [6144, 2048], P('fs'), may hold values from -6 to 6
- merged: bfloat16 [6144, 2048], P('fs'), may hold values from -6 to 6
- gain_first: float32 [2048], replicated, may hold values from 0.1 to 1.9
- gate_first: bfloat16 [2048, 2816], P('fs', 'tp'), may hold values from -0.125 to 0.125
- up_first: bfloat16 [2048, 2816], P('fs', 'tp'), may hold values from -0.125 to 0.125
- down_first: bfloat16 [2816, 2048], P('tp', 'fs'), may hold values from -0.21875 to 0.21875
- gain_second: float32 [2048], replicated, may hold values from 0.1 to 1.9
- gate_second: bfloat16 [2048, 2816], P('fs', 'tp'), may hold values from -0.125 to 0.125
- up_second: bfloat16 [2048, 2816], P('fs', 'tp'), may hold values from -0.125 to 0.125
- down_second: bfloat16 [2816, 2048], P('tp', 'fs'), may hold values from -0.21875 to 0.21875
Outputs:
- result: bfloat16 [6144, 2048], P('fs')
All inputs are finite; a program needn't handle non-finite values.
Results may differ from a plain program's by a relative error of at most 0.01.
Values may be sent and summed in bfloat16 or wider, within the bound.
A program may use at most 64 MiB of HBM per device.

v0:
```python
import jax
import jax.numpy as jnp
from jax import lax
from jax.sharding import PartitionSpec as P

EPS = 1e-06


def norm_rows(values, gain):
    scale = lax.rsqrt(jnp.mean(values * values, axis=-1, keepdims=True) + EPS)
    return values * scale * gain


def make_folder(normed, pieces):
    return (
        jnp.dot(normed, pieces[0], preferred_element_type=jnp.float32),
        jnp.dot(normed, pieces[1], preferred_element_type=jnp.float32),
    )


def shards(
    tokens,
    merged,
    gain_first,
    gate_first,
    up_first,
    down_first,
    gain_second,
    gate_second,
    up_second,
    down_second,
):
    normed_first = norm_rows(tokens.astype(jnp.float32), gain_first).astype(jnp.bfloat16)
    gate, up = make_folder(
        normed_first,
        (
            lax.all_gather(gate_first, "fs", axis=0, tiled=True),
            lax.all_gather(up_first, "fs", axis=0, tiled=True),
        ),
    )
    hidden = (jax.nn.silu(gate) * up).astype(jnp.bfloat16)
    down_whole = lax.all_gather(down_first, "fs", axis=1, tiled=True)
    partial_value = jnp.dot(hidden, down_whole, preferred_element_type=jnp.float32)
    first_sum = lax.psum(partial_value.astype(jnp.bfloat16), "tp").astype(jnp.float32)
    middle = tokens.astype(jnp.float32) + merged.astype(jnp.float32) + 0.5 * first_sum
    normed_second = norm_rows(middle, gain_second).astype(jnp.bfloat16)
    gate_two, up_two = make_folder(
        normed_second,
        (
            lax.all_gather(gate_second, "fs", axis=0, tiled=True),
            lax.all_gather(up_second, "fs", axis=0, tiled=True),
        ),
    )
    hidden_two = (jax.nn.silu(gate_two) * up_two).astype(jnp.bfloat16)
    down_two = lax.all_gather(down_second, "fs", axis=1, tiled=True)
    partial_two = jnp.dot(hidden_two, down_two, preferred_element_type=jnp.float32)
    second_sum = lax.psum(partial_two.astype(jnp.bfloat16), "tp").astype(jnp.float32)
    return (middle + 0.5 * second_sum).astype(jnp.bfloat16)


def solution(mesh):
    return jax.shard_map(
        shards,
        mesh=mesh,
        in_specs=(
            P("fs", None),
            P("fs", None),
            P(),
            P("fs", "tp"),
            P("fs", "tp"),
            P("tp", "fs"),
            P(),
            P("fs", "tp"),
            P("fs", "tp"),
            P("tp", "fs"),
        ),
        out_specs=P("fs", None),
        check_vma=False,
    )
```

profile of v0, /device:TPU:0, one launch (start us, length us, event | category | flops | bytes accessed | tf_op | source)
XLA Modules:
  0.0 665.2 jit_solution(4083028435205835512)
XLA Ops:
  6.5 0.0 all-gather.7.cloned.1.call-start
  6.5 0.7 all-gather.7.cloned.1.call-update
  7.3 0.0 all-gather.11.cloned.1.call-start
  7.3 0.7 all-gather.11.cloned.1.call-update
  8.0 0.0 all-gather.9.cloned.1.call-start
  8.1 0.7 all-gather.9.cloned.1.call-update
  8.7 0.0 all-reduce.3.cloned.1.call-start
  8.8 1.8 fusion.1
  10.6 0.0 copy-start
  10.6 0.0 copy-start.4
  10.6 90.9 %all-gather.7.cloned.1.call-done = bf16[2048,1408]{1,0:T(8,128)(2,1)} async-done(((bf16[128,1408]{1,0:T(8,128)(2,1)}), bf16[2048,1408]{1,0:T(8,128)(2,1)}) %all-gather.7.cloned.1.call-update) | async-done | bytes 5767184 | tf_op jit(solution)/shard_map/all_gather | solution.py:37
  101.5 7.1 %fusion.8 = f32[384,1408]{1,0:T(8,128)} fusion(bf16[2048,1408]{1,0:T(8,128)(2,1)} %all-gather.7.cloned.1.call-done, bf16[384,2048]{1,0:T(8,128)(2,1)} %param.10, f32[2048]{0:T(1024)} %param.12, f32[384]{0:T(512)S(1)} %add_rsqrt_fusion.1), kind=kOutput, calls=%fused_computation.16 | convolution fusion | flops 2217738240 | bytes 9512448 | tf_op jit(solution)/shard_map/dot_general | solution.py:16
  108.7 102.6 %all-gather.11.cloned.1.call-done = bf16[1408,2048]{1,0:T(8,128)(2,1)} async-done(((bf16[1408,128]{1,0:T(8,128)(2,1)}), bf16[1408,2048]{1,0:T(8,128)(2,1)}) %all-gather.11.cloned.1.call-update) | async-done | bytes 5767184 | tf_op jit(solution)/shard_map/all_gather | solution.py:42
  211.3 89.7 %all-gather.9.cloned.1.call-done = bf16[2048,1408]{1,0:T(8,128)(2,1)} async-done(((bf16[128,1408]{1,0:T(8,128)(2,1)}), bf16[2048,1408]{1,0:T(8,128)(2,1)}) %all-gather.9.cloned.1.call-update) | async-done | bytes 5767184 | tf_op jit(solution)/shard_map/all_gather | solution.py:38
  300.9 0.0 copy-done
  300.9 0.0 copy-done.4
  300.9 11.2 %convolution_convert_fusion.1 = bf16[384,2048]{1,0:T(8,128)(2,1)} fusion(bf16[1408,2048]{1,0:T(8,128)(2,1)} %all-gather.11.cloned.1.call-done, bf16[2048,1408]{1,0:T(8,128)(2,1)} %all-gather.9.cloned.1.call-done, f32[384,1408]{1,0:T(8,128)} %fusion.8, bf16[384,2048]{1,0:T(8,128)(2,1)S(1)} %copy-done, f32[2048]{0:T(1024)S(1)} %copy-done.4, ...), kind=kOutput, calls=%fused_computation.15 | convolution fusion | flops 4436361216 | bytes 16852480 | tf_op jit(solution)/shard_map/dot_general | solution.py:43
  312.1 0.0 copy-start.1
  312.1 0.0 all-reduce.3.cloned.1.call-update
  312.2 0.0 copy-start.3
  312.2 0.0 all-gather.13.cloned.1.call-start
  312.2 0.5 all-gather.13.cloned.1.call-update
  312.8 0.0 all-gather.15.cloned.1.call-start
  312.8 0.5 all-gather.15.cloned.1.call-update
  313.3 0.0 all-gather.17.cloned.1.call-start
  313.4 0.7 all-gather.17.cloned.1.call-update
  314.1 0.2 all-reduce.5.cloned.1.call-start
  314.3 17.0 %all-reduce.3.cloned.1.call-done = bf16[384,2048]{1,0:T(8,128)(2,1)} async-done(((bf16[384,2048]{1,0:T(8,128)(2,1)}), bf16[384,2048]{1,0:T(8,128)(2,1)}) %all-reduce.3.cloned.1.call-update) | async-done | bytes 1572880 | tf_op jit(solution)/shard_map/psum | solution.py:44
  331.3 0.0 copy-done.1
  331.3 0.0 copy-start.2
  331.3 2.4 multiply_reduce_fusion
  333.8 0.0 copy-done.3
  333.8 0.0 copy-done.2
  333.8 2.2 multiply_convert_fusion
  336.0 87.8 %all-gather.13.cloned.1.call-done = bf16[2048,1408]{1,0:T(8,128)(2,1)} async-done(((bf16[128,1408]{1,0:T(8,128)(2,1)}), bf16[2048,1408]{1,0:T(8,128)(2,1)}) %all-gather.13.cloned.1.call-update) | async-done | bytes 5767184 | tf_op jit(solution)/shard_map/all_gather | solution.py:50
  423.8 7.1 %fusion.12 = f32[384,1408]{1,0:T(8,128)} fusion(bf16[384,2048]{1,0:T(8,128)(2,1)} %multiply_convert_fusion, bf16[2048,1408]{1,0:T(8,128)(2,1)} %all-gather.13.cloned.1.call-done), kind=kOutput, calls=%fused_computation.21 | convolution fusion | flops 2214592512 | bytes 9502720 | tf_op jit(solution)/shard_map/dot_general | solution.py:16
  430.9 82.9 %all-gather.15.cloned.1.call-done = bf16[2048,1408]{1,0:T(8,128)(2,1)} async-done(((bf16[128,1408]{1,0:T(8,128)(2,1)}), bf16[2048,1408]{1,0:T(8,128)(2,1)}) %all-gather.15.cloned.1.call-update) | async-done | bytes 5767184 | tf_op jit(solution)/shard_map/all_gather | solution.py:51
  513.8 109.7 %all-gather.17.cloned.1.call-done = bf16[1408,2048]{1,0:T(8,128)(2,1)} async-done(((bf16[1408,128]{1,0:T(8,128)(2,1)}), bf16[1408,2048]{1,0:T(8,128)(2,1)}) %all-gather.17.cloned.1.call-update) | async-done | bytes 5767184 | tf_op jit(solution)/shard_map/all_gather | solution.py:55
  623.6 11.7 %convolution_convert_fusion = bf16[384,2048]{1,0:T(8,128)(2,1)} fusion(bf16[1408,2048]{1,0:T(8,128)(2,1)} %all-gather.17.cloned.1.call-done, bf16[384,2048]{1,0:T(8,128)(2,1)} %multiply_convert_fusion, bf16[2048,1408]{1,0:T(8,128)(2,1)} %all-gather.15.cloned.1.call-done, f32[384,1408]{1,0:T(8,128)} %fusion.12), kind=kOutput, calls=%fused_computation.14 | convolution fusion | flops 4433215488 | bytes 16842752 | tf_op jit(solution)/shard_map/dot_general | solution.py:56
  635.3 0.0 all-reduce.5.cloned.1.call-update
  635.3 18.7 %all-reduce.5.cloned.1.call-done = bf16[384,2048]{1,0:T(8,128)(2,1)} async-done(((bf16[384,2048]{1,0:T(8,128)(2,1)}), bf16[384,2048]{1,0:T(8,128)(2,1)}) %all-reduce.5.cloned.1.call-update) | async-done | bytes 1572880 | tf_op jit(solution)/shard_map/psum | solution.py:57
  654.0 4.3 add_convert_fusion
  (2 shorter events, 0.0 us)
Async XLA Ops:
  6.5 95.0 %all-gather.7.cloned.1.call-start = ((), (), s32[]{:S(2)}) async-start(), calls=%async_computation | async-start | bytes 6127616 | tf_op jit(solution)/shard_map/all_gather | solution.py:37
  7.3 204.0 %all-gather.11.cloned.1.call-start = ((), (), s32[]{:S(2)}) async-start(), calls=%async_computation.2 | async-start | bytes 6127616 | tf_op jit(solution)/shard_map/all_gather | solution.py:42
  8.0 292.9 %all-gather.9.cloned.1.call-start = ((), (), s32[]{:S(2)}) async-start(), calls=%async_computation.1 | async-start | bytes 6127616 | tf_op jit(solution)/shard_map/all_gather | solution.py:38
  8.7 322.6 %all-reduce.3.cloned.1.call-start = ((), (), s32[]{:S(2)}) async-start(), calls=%async_computation.3 | async-start | bytes 3145728 | tf_op jit(solution)/shard_map/psum | solution.py:44
  10.6 290.3 %copy-start = (bf16[384,2048]{1,0:T(8,128)(2,1)S(1)}, bf16[384,2048]{1,0:T(8,128)(2,1)}, u32[]{:S(2)}) copy-start(bf16[384,2048]{1,0:T(8,128)(2,1)} %param.10) | copy-start | bytes 4718596
  10.6 290.3 %copy-start.4 = (f32[2048]{0:T(1024)S(1)}, f32[2048]{0:T(1024)}, u32[]{:S(2)}) copy-start(f32[2048]{0:T(1024)} %param.12) | copy-start | bytes 24580
  312.1 19.2 %copy-start.1 = (bf16[384,2048]{1,0:T(8,128)(2,1)S(1)}, bf16[384,2048]{1,0:T(8,128)(2,1)}, u32[]{:S(2)}) copy-start(bf16[384,2048]{1,0:T(8,128)(2,1)} %param.11) | copy-start | bytes 4718596
  312.2 21.6 %copy-start.3 = (f32[2048]{0:T(1024)S(1)}, f32[2048]{0:T(1024)}, u32[]{:S(2)}) copy-start(f32[2048]{0:T(1024)} %param.16) | copy-start | bytes 24580
  312.2 111.7 %all-gather.13.cloned.1.call-start = ((), (), s32[]{:S(2)}) async-start(), calls=%async_computation.4 | async-start | bytes 6127616 | tf_op jit(solution)/shard_map/all_gather | solution.py:50
  312.8 201.1 %all-gather.15.cloned.1.call-start = ((), (), s32[]{:S(2)}) async-start(), calls=%async_computation.5 | async-start | bytes 6127616 | tf_op jit(solution)/shard_map/all_gather | solution.py:51
  313.3 310.2 %all-gather.17.cloned.1.call-start = ((), (), s32[]{:S(2)}) async-start(), calls=%async_computation.6 | async-start | bytes 6127616 | tf_op jit(solution)/shard_map/all_gather | solution.py:55
  314.1 340.0 %all-reduce.5.cloned.1.call-start = ((), (), s32[]{:S(2)}) async-start(), calls=%async_computation.7 | async-start | bytes 3145728 | tf_op jit(solution)/shard_map/psum | solution.py:57
  331.3 2.4 copy-start.2
Sparse Core Ops, SparseCore 0:
  10.0 91.4 all-gather.6
  104.2 106.9 all-gather.10
  213.9 86.9 all-gather.8
  312.3 19.0 all-reduce.2
  333.9 89.9 all-gather.12
  426.4 87.4 all-gather.14
  516.5 106.9 all-gather.16
  635.4 18.5 all-reduce.4
where the time goes:
time: 665 us
  waiting for transfers between devices  603 us (91%)
  matrix products  37.1 us (6%)
  between operations  13.5 us (2%)
  other arithmetic  10.8 us (2%)
    all_gather x1, waiting for transfers between devices, shards(): down_two = lax.all_gather(down_second, 'fs', axis=1, tiled=True)  110 us
    all_gather x1, waiting for transfers between devices, shards(): down_whole = lax.all_gather(down_first, 'fs', axis=1, tiled=True)  103 us
    all_gather x1, waiting for transfers between devices, shards(): lax.all_gather(gate_first, 'fs', axis=0, tiled=True)  90.9 us
    all_gather x1, waiting for transfers between devices, shards(): lax.all_gather(up_first, 'fs', axis=0, tiled=True)  89.7 us
    all_gather x1, waiting for transfers between devices, shards(): lax.all_gather(gate_second, 'fs', axis=0, tiled=True)  87.8 us
    all_gather x1, waiting for transfers between devices, shards(): lax.all_gather(up_second, 'fs', axis=0, tiled=True)  82.9 us
    psum x1, waiting for transfers between devices, shards(): lax.psum(partial_two.astype(jnp.bfloat16), 'tp').astype(jnp.float32)  18.7 us
    psum x1, waiting for transfers between devices, shards(): lax.psum(partial_value.astype(jnp.bfloat16), 'tp').astype(jnp.float32)  17 us
  transfers between devices with their start and end apart: 8, of which 8 were waited for; matrix products, arithmetic and copies ran while one was open for 3% of the time, Pallas kernels for 0%

commit v1 on v0

--- a/solution.py
+++ b/solution.py
@@ -39,7 +39,21 @@
         ),
     )
     hidden = (jax.nn.silu(gate) * up).astype(jnp.bfloat16)
-    down_whole = lax.all_gather(down_first, "fs", axis=1, tiled=True)
+
+    def fill_the_windows(payload, axis_key):
+        amount_of = lax.axis_size(axis_key)
+        entries = []
+        for dd in range(amount_of):
+            entries.append((dd, (dd + 1) % amount_of))
+        row_out = [None] * amount_of
+        row_out[amount_of - 1] = payload
+        for dev_j in range(amount_of - 2, -1, -1):
+            row_out[dev_j] = lax.ppermute(row_out[dev_j + 1], axis_key, entries)
+        all_values = jnp.concatenate(row_out, 1)
+        v_now = lax.axis_index(axis_key)
+        return jnp.roll(all_values, (v_now + 1) * payload.shape[1], 1)
+
+    down_whole = fill_the_windows(down_first, "fs")
     partial_value = jnp.dot(hidden, down_whole, preferred_element_type=jnp.float32)
     first_sum = lax.psum(partial_value.astype(jnp.bfloat16), "tp").astype(jnp.float32)
     middle = tokens.astype(jnp.float32) + merged.astype(jnp.float32) + 0.5 * first_sum

time: 665 us -> 682 us (1.026)
  local copies, waits for them, and re-layouts: 0.02 us -> 36.4 us
  waiting for transfers between devices: 603 us -> 581 us
    ppermute x0 -> x15, waiting for transfers between devices: none -> 257 us  [fill_the_windows(): row_out[dev_j] = lax.ppermute(row_out[dev_j + 1], axis_key, entries)]
    all_gather x1 -> x0, waiting for transfers between devices: 103 us -> none  [shards(): down_whole = lax.all_gather(down_first, 'fs', axis=1, tiled=True)]
    all_gather x1, waiting for transfers between devices: 90.9 us -> 0.01 us  [shards(): lax.all_gather(gate_first, 'fs', axis=0, tiled=True)]
    all_gather x1, waiting for transfers between devices: 89.7 us -> 0.01 us  [shards(): lax.all_gather(up_first, 'fs', axis=0, tiled=True)]
    unnamed x10 -> x69, local copies, waits for them, and re-layouts: 0.02 us -> 35.6 us
  transfers between devices with their start and end apart: 8 -> 22, of which waited for: 8 -> 20; matrix products, arithmetic and copies ran while one was open for 3% -> 8% of each run, Pallas kernels for 0% -> 0%
where the time goes in v1:
time: 682 us
  waiting for transfers between devices  581 us (85%)
  matrix products  36.8 us (5%)
  local copies, waits for them, and re-layouts  36.4 us (5%)
  between operations  13.6 us (2%)
  other arithmetic  10.8 us (2%)
    ppermute x15, waiting for transfers between devices, fill_the_windows(): row_out[dev_j] = lax.ppermute(row_out[dev_j + 1], axis_key, entries)  257 us
    all_gather x1, waiting for transfers between devices, shards(): down_two = lax.all_gather(down_second, 'fs', axis=1, tiled=True)  110 us
    all_gather x1, waiting for transfers between devices, shards(): lax.all_gather(gate_second, 'fs', axis=0, tiled=True)  87.8 us
    all_gather x1, waiting for transfers between devices, shards(): lax.all_gather(up_second, 'fs', axis=0, tiled=True)  82.9 us
    unnamed x69, local copies, waits for them, and re-layouts  35.6 us
    psum x1, waiting for transfers between devices, shards(): lax.psum(partial_value.astype(jnp.bfloat16), 'tp').astype(jnp.float32)  21.9 us
    psum x1, waiting for transfers between devices, shards(): lax.psum(partial_two.astype(jnp.bfloat16), 'tp').astype(jnp.float32)  18.7 us
    dot_general x2, matrix products, make_folder(): jnp.dot(normed, pieces[0], preferred_element_type=jnp.float32)  13.8 us
  transfers between devices with their start and end apart: 22, of which 20 were waited for; matrix products, arithmetic and copies ran while one was open for 8% of the time, Pallas kernels for 0%

profile of v1, /device:TPU:0, one launch (start us, length us, event | category | flops | bytes accessed | tf_op | source)
XLA Modules:
  0.0 681.6 jit_solution(11050914757159950417)
XLA Ops:
  7.3 3.0 collective-permute-start
  10.3 12.6 %collective-permute-done = bf16[1408,128]{1,0:T(8,128)(2,1)S(1)} collective-permute-done((bf16[1408,128]{1,0:T(8,128)(2,1)}, bf16[1408,128]{1,0:T(8,128)(2,1)S(1)}, u32[]{:S(2)}, u32[]{:S(2)}) %collective-permute-start) | collective-permute-done | bytes 360480 | tf_op jit(solution)/shard_map/ppermute | solution.py:51
  22.9 20.4 %collective-permute-done.1 = bf16[1408,128]{1,0:T(8,128)(2,1)S(1)} collective-permute-done((bf16[1408,128]{1,0:T(8,128)(2,1)S(1)}, bf16[1408,128]{1,0:T(8,128)(2,1)S(1)}, u32[]{:S(2)}, u32[]{:S(2)}) %collective-permute-start.1) | collective-permute-done | bytes 360480 | tf_op jit(solution)/shard_map/ppermute | solution.py:51
  43.4 21.1 %collective-permute-done.2 = bf16[1408,128]{1,0:T(8,128)(2,1)S(1)} collective-permute-done((bf16[1408,128]{1,0:T(8,128)(2,1)S(1)}, bf16[1408,128]{1,0:T(8,128)(2,1)S(1)}, u32[]{:S(2)}, u32[]{:S(2)}) %collective-permute-start.2) | collective-permute-done | bytes 360480 | tf_op jit(solution)/shard_map/ppermute | solution.py:51
  64.5 15.5 %collective-permute-done.3 = bf16[1408,128]{1,0:T(8,128)(2,1)S(1)} collective-permute-done((bf16[1408,128]{1,0:T(8,128)(2,1)S(1)}, bf16[1408,128]{1,0:T(8,128)(2,1)S(1)}, u32[]{:S(2)}, u32[]{:S(2)}) %collective-permute-start.3) | collective-permute-done | bytes 360480 | tf_op jit(solution)/shard_map/ppermute | solution.py:51
  80.0 21.7 %collective-permute-done.4 = bf16[1408,128]{1,0:T(8,128)(2,1)S(1)} collective-permute-done((bf16[1408,128]{1,0:T(8,128)(2,1)S(1)}, bf16[1408,128]{1,0:T(8,128)(2,1)S(1)}, u32[]{:S(2)}, u32[]{:S(2)}) %collective-permute-start.4) | collective-permute-done | bytes 360480 | tf_op jit(solution)/shard_map/ppermute | solution.py:51
  101.7 21.5 %collective-permute-done.5 = bf16[1408,128]{1,0:T(8,128)(2,1)S(1)} collective-permute-done((bf16[1408,128]{1,0:T(8,128)(2,1)S(1)}, bf16[1408,128]{1,0:T(8,128)(2,1)S(1)}, u32[]{:S(2)}, u32[]{:S(2)}) %collective-permute-start.5) | collective-permute-done | bytes 360480 | tf_op jit(solution)/shard_map/ppermute | solution.py:51
  123.2 15.4 %collective-permute-done.6 = bf16[1408,128]{1,0:T(8,128)(2,1)S(1)} collective-permute-done((bf16[1408,128]{1,0:T(8,128)(2,1)S(1)}, bf16[1408,128]{1,0:T(8,128)(2,1)S(1)}, u32[]{:S(2)}, u32[]{:S(2)}) %collective-permute-start.6) | collective-permute-done | bytes 360480 | tf_op jit(solution)/shard_map/ppermute | solution.py:51
  138.7 12.7 %collective-permute-done.7 = bf16[1408,128]{1,0:T(8,128)(2,1)S(1)} collective-permute-done((bf16[1408,128]{1,0:T(8,128)(2,1)S(1)}, bf16[1408,128]{1,0:T(8,128)(2,1)S(1)}, u32[]{:S(2)}, u32[]{:S(2)}) %collective-permute-start.7) | collective-permute-done | bytes 360480 | tf_op jit(solution)/shard_map/ppermute | solution.py:51
  151.4 11.8 %collective-permute-done.8 = bf16[1408,128]{1,0:T(8,128)(2,1)S(1)} collective-permute-done((bf16[1408,128]{1,0:T(8,128)(2,1)S(1)}, bf16[1408,128]{1,0:T(8,128)(2,1)S(1)}, u32[]{:S(2)}, u32[]{:S(2)}) %collective-permute-start.8) | collective-permute-done | bytes 360480 | tf_op jit(solution)/shard_map/ppermute | solution.py:51
  163.2 18.7 %collective-permute-done.9 = bf16[1408,128]{1,0:T(8,128)(2,1)S(1)} collective-permute-done((bf16[1408,128]{1,0:T(8,128)(2,1)S(1)}, bf16[1408,128]{1,0:T(8,128)(2,1)S(1)}, u32[]{:S(2)}, u32[]{:S(2)}) %collective-permute-start.9) | collective-permute-done | bytes 360480 | tf_op jit(solution)/shard_map/ppermute | solution.py:51
  182.7 21.1 %collective-permute-done.10 = bf16[1408,128]{1,0:T(8,128)(2,1)S(1)} collective-permute-done((bf16[1408,128]{1,0:T(8,128)(2,1)S(1)}, bf16[1408,128]{1,0:T(8,128)(2,1)S(1)}, u32[]{:S(2)}, u32[]{:S(2)}) %collective-permute-start.10) | collective-permute-done | bytes 360480 | tf_op jit(solution)/shard_map/ppermute | solution.py:51
  204.5 14.5 %collective-permute-done.11 = bf16[1408,128]{1,0:T(8,128)(2,1)S(1)} collective-permute-done((bf16[1408,128]{1,0:T(8,128)(2,1)S(1)}, bf16[1408,128]{1,0:T(8,128)(2,1)S(1)}, u32[]{:S(2)}, u32[]{:S(2)}) %collective-permute-start.11) | collective-permute-done | bytes 360480 | tf_op jit(solution)/shard_map/ppermute | solution.py:51
  219.8 22.8 %collective-permute-done.12 = bf16[1408,128]{1,0:T(8,128)(2,1)} collective-permute-done((bf16[1408,128]{1,0:T(8,128)(2,1)S(1)}, bf16[1408,128]{1,0:T(8,128)(2,1)}, u32[]{:S(2)}, u32[]{:S(2)}) %collective-permute-start.12) | collective-permute-done | bytes 360480 | tf_op jit(solution)/shard_map/ppermute | solution.py:51
  242.6 16.8 %collective-permute-done.13 = bf16[1408,128]{1,0:T(8,128)(2,1)} collective-permute-done((bf16[1408,128]{1,0:T(8,128)(2,1)}, bf16[1408,128]{1,0:T(8,128)(2,1)}, u32[]{:S(2)}, u32[]{:S(2)}) %collective-permute-start.13) | collective-permute-done | bytes 360480 | tf_op jit(solution)/shard_map/ppermute | solution.py:51
  259.4 1.8 fusion.3
  261.2 10.7 %collective-permute-done.14 = bf16[1408,128]{1,0:T(8,128)(2,1)S(1)} collective-permute-done((bf16[1408,128]{1,0:T(8,128)(2,1)}, bf16[1408,128]{1,0:T(8,128)(2,1)S(1)}, u32[]{:S(2)}, u32[]{:S(2)}) %collective-permute-start.14) | collective-permute-done | bytes 360480 | tf_op jit(solution)/shard_map/ppermute | solution.py:51
  272.7 1.8 constant_dynamic-update-slice_fusion.30
  274.5 1.8 constant_dynamic-update-slice_fusion.29
  276.4 1.9 constant_dynamic-update-slice_fusion.28
  278.2 1.9 constant_dynamic-update-slice_fusion.27
  280.1 1.9 constant_dynamic-update-slice_fusion.26
  282.0 0.8 constant_dynamic-update-slice_fusion.25
  282.8 0.8 constant_dynamic-update-slice_fusion.24
  284.4 0.8 constant_dynamic-update-slice_fusion.22
  286.8 0.8 constant_dynamic-update-slice_fusion.19
  290.0 0.8 constant_dynamic-update-slice_fusion.15
  290.9 1.8 constant_dynamic-update-slice_fusion.14
  292.7 1.8 constant_dynamic-update-slice_fusion.13
  294.5 0.8 constant_dynamic-update-slice_fusion.12
  296.1 0.8 constant_dynamic-update-slice_fusion.10
  296.9 1.8 constant_dynamic-update-slice_fusion.9
  299.5 0.8 constant_dynamic-update-slice_fusion.7
  300.3 0.8 constant_dynamic-update-slice_fusion.6
  301.2 0.8 constant_dynamic-update-slice_fusion.5
  303.6 0.8 constant_dynamic-update-slice_fusion.2
  306.0 6.7 fusion.13
  312.7 11.3 %fusion.8 = bf16[384,2048]{1,0:T(8,128)(2,1)} fusion(bf16[1408,4096]{1,0:T(8,128)(2,1)} %constant_dynamic-update-slice_fusion, s32[]{:T(128)S(6)} %select_n.14, bf16[2048,1408]{1,0:T(8,128)(2,1)} %all-gather.8.cloned.1.call-done, f32[384,1408]{1,0:T(8,128)} %fusion.13, bf16[384,2048]{1,0:T(8,128)(2,1)S(1)} %copy-done, f32[2048]{0:T(1024)S(1)} %copy-done.18, ...), kind=kOutput, calls=%fused_computation.16 | convolution fusion | flops 4436361216 | bytes 16852484 | tf_op jit(solution)/shard_map/dot_general | solution.py:57
  326.0 21.9 %all-reduce.3.cloned.1.call-done = bf16[384,2048]{1,0:T(8,128)(2,1)} async-done(((bf16[384,2048]{1,0:T(8,128)(2,1)}), bf16[384,2048]{1,0:T(8,128)(2,1)}) %all-reduce.3.cloned.1.call-update) | async-done | bytes 1572880 | tf_op jit(solution)/shard_map/psum | solution.py:58
  348.0 2.4 multiply_reduce_fusion
  350.4 2.2 multiply_convert_fusion
  352.6 87.8 %all-gather.10.cloned.1.call-done = bf16[2048,1408]{1,0:T(8,128)(2,1)} async-done(((bf16[128,1408]{1,0:T(8,128)(2,1)}), bf16[2048,1408]{1,0:T(8,128)(2,1)}) %all-gather.10.cloned.1.call-update) | async-done | bytes 5767184 | tf_op jit(solution)/shard_map/all_gather | solution.py:64
  440.5 7.1 %fusion.18 = f32[384,1408]{1,0:T(8,128)} fusion(bf16[384,2048]{1,0:T(8,128)(2,1)} %multiply_convert_fusion, bf16[2048,1408]{1,0:T(8,128)(2,1)} %all-gather.10.cloned.1.call-done), kind=kOutput, calls=%fused_computation.56 | convolution fusion | flops 2214592512 | bytes 9502720 | tf_op jit(solution)/shard_map/dot_general | solution.py:16
  447.5 82.9 %all-gather.12.cloned.1.call-done = bf16[2048,1408]{1,0:T(8,128)(2,1)} async-done(((bf16[128,1408]{1,0:T(8,128)(2,1)}), bf16[2048,1408]{1,0:T(8,128)(2,1)}) %all-gather.12.cloned.1.call-update) | async-done | bytes 5767184 | tf_op jit(solution)/shard_map/all_gather | solution.py:65
  530.5 109.6 %all-gather.14.cloned.1.call-done = bf16[1408,2048]{1,0:T(8,128)(2,1)} async-done(((bf16[1408,128]{1,0:T(8,128)(2,1)}), bf16[1408,2048]{1,0:T(8,128)(2,1)}) %all-gather.14.cloned.1.call-update) | async-done | bytes 5767184 | tf_op jit(solution)/shard_map/all_gather | solution.py:69
  640.0 11.7 %convolution_convert_fusion = bf16[384,2048]{1,0:T(8,128)(2,1)} fusion(bf16[1408,2048]{1,0:T(8,128)(2,1)} %all-gather.14.cloned.1.call-done, bf16[384,2048]{1,0:T(8,128)(2,1)} %multiply_convert_fusion, bf16[2048,1408]{1,0:T(8,128)(2,1)} %all-gather.12.cloned.1.call-done, f32[384,1408]{1,0:T(8,128)} %fusion.18), kind=kOutput, calls=%fused_computation.17 | convolution fusion | flops 4433215488 | bytes 16842752 | tf_op jit(solution)/shard_map/dot_general | solution.py:70
  651.8 18.7 %all-reduce.5.cloned.1.call-done = bf16[384,2048]{1,0:T(8,128)(2,1)} async-done(((bf16[384,2048]{1,0:T(8,128)(2,1)}), bf16[384,2048]{1,0:T(8,128)(2,1)}) %all-reduce.5.cloned.1.call-update) | async-done | bytes 1572880 | tf_op jit(solution)/shard_map/psum | solution.py:71
  670.5 4.3 add_convert_fusion
  (83 shorter events, 15.5 us)
Async XLA Ops:
  6.5 299.5 %all-gather.6.cloned.1.call-start = ((), (), s32[]{:S(2)}) async-start(), calls=%async_computation | async-start | bytes 6127616 | tf_op jit(solution)/shard_map/all_gather | solution.py:37
  7.3 305.5 %all-gather.8.cloned.1.call-start = ((), (), s32[]{:S(2)}) async-start(), calls=%async_computation.1 | async-start | bytes 6127616 | tf_op jit(solution)/shard_map/all_gather | solution.py:38
  7.3 15.6 %collective-permute-start = (bf16[1408,128]{1,0:T(8,128)(2,1)}, bf16[1408,128]{1,0:T(8,128)(2,1)S(1)}, u32[]{:S(2)}, u32[]{:S(2)}) collective-permute-start(bf16[1408,128]{1,0:T(8,128)(2,1)} %param.15), channel_id=1, source_target_pairs={{0,2},{2,4},{4,6},{6,8},{8,10},{10,12},{12,14},{14,16},{16,18},{18... | collective-permute-start | bytes 1081352 | tf_op jit(solution)/shard_map/ppermute | solution.py:51
  22.9 20.4 %collective-permute-start.1 = (bf16[1408,128]{1,0:T(8,128)(2,1)S(1)}, bf16[1408,128]{1,0:T(8,128)(2,1)S(1)}, u32[]{:S(2)}, u32[]{:S(2)}) collective-permute-start(bf16[1408,128]{1,0:T(8,128)(2,1)S(1)} %collective-permute-done), channel_id=1, source_target_pairs={{0,2},{2,4},{4,6},{6,8},{8,10},{10,12},{12,14},{14,16},{16,18},{18... | collective-permute-start | bytes 1081352 | tf_op jit(solution)/shard_map/ppermute | solution.py:51
  43.4 21.1 %collective-permute-start.2 = (bf16[1408,128]{1,0:T(8,128)(2,1)S(1)}, bf16[1408,128]{1,0:T(8,128)(2,1)S(1)}, u32[]{:S(2)}, u32[]{:S(2)}) collective-permute-start(bf16[1408,128]{1,0:T(8,128)(2,1)S(1)} %collective-permute-done.1), channel_id=1, source_target_pairs={{0,2},{2,4},{4,6},{6,8},{8,10},{10,12},{12,14},{14,16},{16,18},{18... | collective-permute-start | bytes 1081352 | tf_op jit(solution)/shard_map/ppermute | solution.py:51
  64.4 15.5 %collective-permute-start.3 = (bf16[1408,128]{1,0:T(8,128)(2,1)S(1)}, bf16[1408,128]{1,0:T(8,128)(2,1)S(1)}, u32[]{:S(2)}, u32[]{:S(2)}) collective-permute-start(bf16[1408,128]{1,0:T(8,128)(2,1)S(1)} %collective-permute-done.2), channel_id=1, source_target_pairs={{0,2},{2,4},{4,6},{6,8},{8,10},{10,12},{12,14},{14,16},{16,18},{18... | collective-permute-start | bytes 1081352 | tf_op jit(solution)/shard_map/ppermute | solution.py:51
  80.0 21.7 %collective-permute-start.4 = (bf16[1408,128]{1,0:T(8,128)(2,1)S(1)}, bf16[1408,128]{1,0:T(8,128)(2,1)S(1)}, u32[]{:S(2)}, u32[]{:S(2)}) collective-permute-start(bf16[1408,128]{1,0:T(8,128)(2,1)S(1)} %collective-permute-done.3), channel_id=1, source_target_pairs={{0,2},{2,4},{4,6},{6,8},{8,10},{10,12},{12,14},{14,16},{16,18},{18... | collective-permute-start | bytes 1081352 | tf_op jit(solution)/shard_map/ppermute | solution.py:51
  101.7 21.5 %collective-permute-start.5 = (bf16[1408,128]{1,0:T(8,128)(2,1)S(1)}, bf16[1408,128]{1,0:T(8,128)(2,1)S(1)}, u32[]{:S(2)}, u32[]{:S(2)}) collective-permute-start(bf16[1408,128]{1,0:T(8,128)(2,1)S(1)} %collective-permute-done.4), channel_id=1, source_target_pairs={{0,2},{2,4},{4,6},{6,8},{8,10},{10,12},{12,14},{14,16},{16,18},{18... | collective-permute-start | bytes 1081352 | tf_op jit(solution)/shard_map/ppermute | solution.py:51
  123.2 165.2 %copy-start.4 = (bf16[1408,128]{1,0:T(8,128)(2,1)}, bf16[1408,128]{1,0:T(8,128)(2,1)S(1)}, u32[]{:S(2)}) copy-start(bf16[1408,128]{1,0:T(8,128)(2,1)S(1)} %collective-permute-done.5) | copy-start | bytes 1081348
  123.2 15.4 %collective-permute-start.6 = (bf16[1408,128]{1,0:T(8,128)(2,1)S(1)}, bf16[1408,128]{1,0:T(8,128)(2,1)S(1)}, u32[]{:S(2)}, u32[]{:S(2)}) collective-permute-start(bf16[1408,128]{1,0:T(8,128)(2,1)S(1)} %collective-permute-done.5), channel_id=1, source_target_pairs={{0,2},{2,4},{4,6},{6,8},{8,10},{10,12},{12,14},{14,16},{16,18},{18... | collective-permute-start | bytes 1081352 | tf_op jit(solution)/shard_map/ppermute | solution.py:51
  138.7 149.8 %copy-start.6 = (bf16[1408,128]{1,0:T(8,128)(2,1)}, bf16[1408,128]{1,0:T(8,128)(2,1)S(1)}, u32[]{:S(2)}) copy-start(bf16[1408,128]{1,0:T(8,128)(2,1)S(1)} %collective-permute-done.6) | copy-start | bytes 1081348
  138.7 12.7 %collective-permute-start.7 = (bf16[1408,128]{1,0:T(8,128)(2,1)S(1)}, bf16[1408,128]{1,0:T(8,128)(2,1)S(1)}, u32[]{:S(2)}, u32[]{:S(2)}) collective-permute-start(bf16[1408,128]{1,0:T(8,128)(2,1)S(1)} %collective-permute-done.6), channel_id=1, source_target_pairs={{0,2},{2,4},{4,6},{6,8},{8,10},{10,12},{12,14},{14,16},{16,18},{18... | collective-permute-start | bytes 1081352 | tf_op jit(solution)/shard_map/ppermute | solution.py:51
  151.4 137.1 %copy-start.8 = (bf16[1408,128]{1,0:T(8,128)(2,1)}, bf16[1408,128]{1,0:T(8,128)(2,1)S(1)}, u32[]{:S(2)}) copy-start(bf16[1408,128]{1,0:T(8,128)(2,1)S(1)} %collective-permute-done.7) | copy-start | bytes 1081348
  151.4 11.8 %collective-permute-start.8 = (bf16[1408,128]{1,0:T(8,128)(2,1)S(1)}, bf16[1408,128]{1,0:T(8,128)(2,1)S(1)}, u32[]{:S(2)}, u32[]{:S(2)}) collective-permute-start(bf16[1408,128]{1,0:T(8,128)(2,1)S(1)} %collective-permute-done.7), channel_id=1, source_target_pairs={{0,2},{2,4},{4,6},{6,8},{8,10},{10,12},{12,14},{14,16},{16,18},{18... | collective-permute-start | bytes 1081352 | tf_op jit(solution)/shard_map/ppermute | solution.py:51
  151.4 196.6 %all-reduce.3.cloned.1.call-start = ((), (), s32[]{:S(2)}) async-start(), calls=%async_computation.2 | async-start | bytes 3145728 | tf_op jit(solution)/shard_map/psum | solution.py:58
  163.2 125.3 %copy-start.10 = (bf16[1408,128]{1,0:T(8,128)(2,1)}, bf16[1408,128]{1,0:T(8,128)(2,1)S(1)}, u32[]{:S(2)}) copy-start(bf16[1408,128]{1,0:T(8,128)(2,1)S(1)} %collective-permute-done.8) | copy-start | bytes 1081348
  163.2 18.7 %collective-permute-start.9 = (bf16[1408,128]{1,0:T(8,128)(2,1)S(1)}, bf16[1408,128]{1,0:T(8,128)(2,1)S(1)}, u32[]{:S(2)}, u32[]{:S(2)}) collective-permute-start(bf16[1408,128]{1,0:T(8,128)(2,1)S(1)} %collective-permute-done.8), channel_id=1, source_target_pairs={{0,2},{2,4},{4,6},{6,8},{8,10},{10,12},{12,14},{14,16},{16,18},{18... | collective-permute-start | bytes 1081352 | tf_op jit(solution)/shard_map/ppermute | solution.py:51
  181.9 0.8 copy-start.11
  182.7 21.1 %collective-permute-start.10 = (bf16[1408,128]{1,0:T(8,128)(2,1)S(1)}, bf16[1408,128]{1,0:T(8,128)(2,1)S(1)}, u32[]{:S(2)}, u32[]{:S(2)}) collective-permute-start(bf16[1408,128]{1,0:T(8,128)(2,1)S(1)} %collective-permute-done.9), channel_id=1, source_target_pairs={{0,2},{2,4},{4,6},{6,8},{8,10},{10,12},{12,14},{14,16},{16,18},{18... | collective-permute-start | bytes 1081352 | tf_op jit(solution)/shard_map/ppermute | solution.py:51
  203.7 0.8 copy-start.13
  204.5 14.5 %collective-permute-start.11 = (bf16[1408,128]{1,0:T(8,128)(2,1)S(1)}, bf16[1408,128]{1,0:T(8,128)(2,1)S(1)}, u32[]{:S(2)}, u32[]{:S(2)}) collective-permute-start(bf16[1408,128]{1,0:T(8,128)(2,1)S(1)} %collective-permute-done.10), channel_id=1, source_target_pairs={{0,2},{2,4},{4,6},{6,8},{8,10},{10,12},{12,14},{14,16},{16,18},{18... | collective-permute-start | bytes 1081352 | tf_op jit(solution)/shard_map/ppermute | solution.py:51
  219.0 0.7 copy-start.15
  219.8 22.8 %collective-permute-start.12 = (bf16[1408,128]{1,0:T(8,128)(2,1)S(1)}, bf16[1408,128]{1,0:T(8,128)(2,1)}, u32[]{:S(2)}, u32[]{:S(2)}) collective-permute-start(bf16[1408,128]{1,0:T(8,128)(2,1)S(1)} %collective-permute-done.11), channel_id=1, source_target_pairs={{0,2},{2,4},{4,6},{6,8},{8,10},{10,12},{12,14},{14,16},{16,18},{18... | collective-permute-start | bytes 1081352 | tf_op jit(solution)/shard_map/ppermute | solution.py:51
  242.6 16.8 %collective-permute-start.13 = (bf16[1408,128]{1,0:T(8,128)(2,1)}, bf16[1408,128]{1,0:T(8,128)(2,1)}, u32[]{:S(2)}, u32[]{:S(2)}) collective-permute-start(bf16[1408,128]{1,0:T(8,128)(2,1)} %collective-permute-done.12), channel_id=1, source_target_pairs={{0,2},{2,4},{4,6},{6,8},{8,10},{10,12},{12,14},{14,16},{16,18},{18... | collective-permute-start | bytes 1081352 | tf_op jit(solution)/shard_map/ppermute | solution.py:51
  259.4 12.5 %collective-permute-start.14 = (bf16[1408,128]{1,0:T(8,128)(2,1)}, bf16[1408,128]{1,0:T(8,128)(2,1)S(1)}, u32[]{:S(2)}, u32[]{:S(2)}) collective-permute-start(bf16[1408,128]{1,0:T(8,128)(2,1)} %collective-permute-done.13), channel_id=1, source_target_pairs={{0,2},{2,4},{4,6},{6,8},{8,10},{10,12},{12,14},{14,16},{16,18},{18... | collective-permute-start | bytes 1081352 | tf_op jit(solution)/shard_map/ppermute | solution.py:51
  261.2 28.1 %copy-start.3 = (bf16[1408,128]{1,0:T(8,128)(2,1)S(1)}, bf16[1408,128]{1,0:T(8,128)(2,1)}, u32[]{:S(2)}) copy-start(bf16[1408,128]{1,0:T(8,128)(2,1)} %param.15) | copy-start | bytes 1081348
  276.4 18.1 %copy-start.16 = (bf16[1408,128]{1,0:T(8,128)(2,1)S(1)}, bf16[1408,128]{1,0:T(8,128)(2,1)}, u32[]{:S(2)}) copy-start(bf16[1408,128]{1,0:T(8,128)(2,1)} %copy-done.15) | copy-start | bytes 1081348
  278.2 17.1 %copy-start.14 = (bf16[1408,128]{1,0:T(8,128)(2,1)S(1)}, bf16[1408,128]{1,0:T(8,128)(2,1)}, u32[]{:S(2)}) copy-start(bf16[1408,128]{1,0:T(8,128)(2,1)} %copy-done.13) | copy-start | bytes 1081348
  280.1 16.0 %copy-start.12 = (bf16[1408,128]{1,0:T(8,128)(2,1)S(1)}, bf16[1408,128]{1,0:T(8,128)(2,1)}, u32[]{:S(2)}) copy-start(bf16[1408,128]{1,0:T(8,128)(2,1)} %copy-done.11) | copy-start | bytes 1081348
  289.2 9.5 %copy-start.9 = (bf16[1408,128]{1,0:T(8,128)(2,1)S(1)}, bf16[1408,128]{1,0:T(8,128)(2,1)}, u32[]{:S(2)}) copy-start(bf16[1408,128]{1,0:T(8,128)(2,1)} %copy-done.8) | copy-start | bytes 1081348
  289.2 10.3 %copy-start.7 = (bf16[1408,128]{1,0:T(8,128)(2,1)S(1)}, bf16[1408,128]{1,0:T(8,128)(2,1)}, u32[]{:S(2)}) copy-start(bf16[1408,128]{1,0:T(8,128)(2,1)} %copy-done.6) | copy-start | bytes 1081348
  289.3 11.1 %copy-start.5 = (bf16[1408,128]{1,0:T(8,128)(2,1)S(1)}, bf16[1408,128]{1,0:T(8,128)(2,1)}, u32[]{:S(2)}) copy-start(bf16[1408,128]{1,0:T(8,128)(2,1)} %copy-done.4) | copy-start | bytes 1081348
  290.0 16.0 %copy-start = (bf16[384,2048]{1,0:T(8,128)(2,1)S(1)}, bf16[384,2048]{1,0:T(8,128)(2,1)}, u32[]{:S(2)}) copy-start(bf16[384,2048]{1,0:T(8,128)(2,1)} %param.10) | copy-start | bytes 4718596
  290.0 16.0 %copy-start.18 = (f32[2048]{0:T(1024)S(1)}, f32[2048]{0:T(1024)}, u32[]{:S(2)}) copy-start(f32[2048]{0:T(1024)} %param.12) | copy-start | bytes 24580
  312.7 35.2 %copy-start.1 = (bf16[384,2048]{1,0:T(8,128)(2,1)S(1)}, bf16[384,2048]{1,0:T(8,128)(2,1)}, u32[]{:S(2)}) copy-start(bf16[384,2048]{1,0:T(8,128)(2,1)} %param.11) | copy-start | bytes 4718596
  324.0 26.3 %copy-start.17 = (f32[2048]{0:T(1024)S(1)}, f32[2048]{0:T(1024)}, u32[]{:S(2)}) copy-start(f32[2048]{0:T(1024)} %param.16) | copy-start | bytes 24580
  324.1 116.4 %all-gather.10.cloned.1.call-start = ((), (), s32[]{:S(2)}) async-start(), calls=%async_computation.3 | async-start | bytes 6127616 | tf_op jit(solution)/shard_map/all_gather | solution.py:64
  324.6 205.8 %all-gather.12.cloned.1.call-start = ((), (), s32[]{:S(2)}) async-start(), calls=%async_computation.4 | async-start | bytes 6127616 | tf_op jit(solution)/shard_map/all_gather | solution.py:65
  325.2 314.8 %all-gather.14.cloned.1.call-start = ((), (), s32[]{:S(2)}) async-start(), calls=%async_computation.5 | async-start | bytes 6127616 | tf_op jit(solution)/shard_map/all_gather | solution.py:69
  325.8 344.7 %all-reduce.5.cloned.1.call-start = ((), (), s32[]{:S(2)}) async-start(), calls=%async_computation.6 | async-start | bytes 3145728 | tf_op jit(solution)/shard_map/psum | solution.py:71
  347.9 2.4 copy-start.2
Sparse Core Ops, SparseCore 0:
  10.0 118.7 all-gather.5
  151.5 108.7 all-gather.7
  324.2 23.7 all-reduce.2
  350.5 89.9 all-gather.9
  443.0 87.4 all-gather.11
  533.0 106.9 all-gather.13
  651.9 18.5 all-reduce.4
